TPU v7x, 32 devices: a whole 2x2x4 slice. The times are simulated.
32 devices in a mesh: grp: 2 (over y), kv: 4 (over z), tp: 4 (over x, core).
Axes of the slice: x: 2, y: 2, z: 4, core: 2. Of those that a mesh axis runs over, the one named last changes fastest.
Arguments:
- piece_rows: bfloat16 [512, 2048], P(('grp', 'kv')), parts along dimension 0, may hold values from -6 to 6
- dec_rows: bfloat16 [16, 2048], P(('grp', 'kv')), parts along dimension 0, may hold values from -6 to 6
- norm_gain: float32 [2048], replicated, may hold values from 0.1 to 1.9
- w_query: bfloat16 [2048, 1024], P(None, 'tp'), may hold values from -0.25 to 0.25
- w_key: bfloat16 [2048, 256], P(None, 'tp'), may hold values from -0.125 to 0.125
- w_value: bfloat16 [2048, 256], P(None, 'tp'), may hold values from -0.125 to 0.125
- w_forget: bfloat16 [2048, 16], P(None, 'tp'), may hold values from -0.125 to 0.125
- forget_bias: float32 [16], P('tp'), may hold values from 3 to 12
- piece_decay: float32 [16, 512], P('tp', ('grp', 'kv')), parts along dimension 1, may hold values from -3 to 0
- cache_kv: bfloat16 [6144, 4, 128], P(('grp', 'kv'), 'tp'), parts along dimension 0, may hold values from -150 to 150
- cache_gate: float32 [16, 6144], P('tp', ('grp', 'kv')), parts along dimension 1, may hold values from -156.6 to 0, as said below
- dec_cache: bfloat16 [16, 3072, 4, 128], P(('grp', 'kv'), None, 'tp'), parts along dimension 0, may hold values from -150 to 150
- dec_gate: float32 [16, 16, 3072], P(('grp', 'kv'), 'tp'), parts along dimension 0, may hold values from -156.6 to 0, as said below
- dec_lengths: int32 [16], P(('grp', 'kv')), parts along dimension 0, may hold values from 1 to 3072, as said below
- w_out: bfloat16 [1024, 2048], P(None, 'tp'), may hold values from -0.75 to 0.75
Outputs:
- piece_out: bfloat16 [512, 2048], P(('grp', 'kv'), 'tp'), parts along dimension 0
- dec_out: bfloat16 [16, 2048], P(('grp', 'kv'), 'tp'), parts along dimension 0
There are 2 independent parts, one for each index of `grp`. A program takes and returns all parts, laid end to end along the dimension named above; an argument that names none is the same for every part. Nothing has to cross between parts.
Inputs may be any that keep to these rules, and one draw needn't show every extreme that they name: `cache_gate`: each head's values never fall from one position to the next and are 0 at the last cached position. `dec_gate`: each sequence's and head's values never rise from one position to the next. Sequence b's cache holds its first dec_lengths[b] positions; in each part some sequence holds 3072.
All inputs are finite; a program needn't handle non-finite values.
Results may differ from a plain program's by a relative error of at most 0.006.
The roundings to bfloat16 on the way count: a program that leaves them out, or rounds other values in their place, can miss the bound.
Values may be sent and summed in bfloat16 or wider, within the bound.
A program may use at most 64 MiB of HBM per device.

v0:
```python
import jax
import jax.numpy as jnp
from jax import lax
from jax.sharding import PartitionSpec as P


def carried_in(array, axis, combine, identity):
    length, mine = (lax.axis_size(axis), lax.axis_index(axis))
    everything = lax.all_gather(array, axis)
    start = jnp.broadcast_to(jnp.asarray(identity, array.dtype), array.shape)

    def lap(k, before):
        reached = k < mine
        new = combine(before, everything[k])
        return jnp.where(reached, new, before)

    return lax.fori_loop(0, length, lap, start)


def norm_rows(rows, gain):
    wide = rows.astype(jnp.float32)
    scale = lax.rsqrt(jnp.mean(wide * wide, axis=-1, keepdims=True) + 1e-06)
    return (wide * scale * gain).astype(jnp.bfloat16)


def add_terms(earlier, later):
    return earlier + later


def merge_state(state, part):
    peak, total, numer = state
    new_peak, new_total, new_numer = part
    highest = jnp.maximum(peak, new_peak)
    keep = jnp.exp(peak - highest)
    fresh = jnp.exp(new_peak - highest)
    return (
        highest,
        total * keep + new_total * fresh,
        numer * keep[..., None] + new_numer * fresh[..., None],
    )


def group_partial(query, query_index, group_kv, group_bias, group, past_rows, new_rows):
    head_width = query.shape[-1]
    keys = group_kv[..., :head_width]
    values = group_kv[..., head_width:]
    score = jnp.einsum("bkgd,nkd->bkgn", query, keys, preferred_element_type=jnp.float32)
    score = score * head_width ** (-0.5) + group_bias[None]
    rank = jnp.arange(group_kv.shape[0], dtype=jnp.int32)
    new_index = group * new_rows + rank - past_rows
    visible = (rank < past_rows)[None, :] | (new_index[None, :] <= query_index[:, None])
    score = jnp.where(visible[:, None, None, :], score, -jnp.inf)
    peak = jnp.max(score, axis=-1)
    weight = jnp.exp(score - peak[..., None])
    total = jnp.sum(weight, axis=-1)
    numer = jnp.einsum(
        "bkgn,nkd->bkgd", weight.astype(jnp.bfloat16), values, preferred_element_type=jnp.float32
    )
    return (peak, total, numer)


def decode_attention(query, new_key, new_value, new_gate, cache, gate, lengths):
    seqs, pairs_here, group_size, head_width = query.shape
    span = cache.shape[1]
    keys = cache[..., :head_width]
    values = cache[..., head_width:]
    target_location = jnp.arange(span, dtype=jnp.int32)
    last_gate = jnp.sum(
        jnp.where(target_location[None, None, :] == lengths[:, None, None] - 1, gate, 0.0), axis=-1
    )
    score = jnp.einsum(
        "skgd,slkd->skgl", query, keys, preferred_element_type=jnp.float32
    ) * head_width ** (-0.5)
    score = score - gate.reshape(seqs, pairs_here, group_size, span)
    score = jnp.where(
        (target_location[None, :] < lengths[:, None])[:, None, None, :], score, -jnp.inf
    )
    own = jnp.einsum(
        "skgd,skd->skg", query, new_key, preferred_element_type=jnp.float32
    ) * head_width ** (-0.5)
    own = own - (last_gate + new_gate).reshape(seqs, pairs_here, group_size)
    peak = jnp.maximum(jnp.max(score, axis=-1), own)
    weight = jnp.exp(score - peak[..., None])
    own_weight = jnp.exp(own - peak)
    total = jnp.sum(weight, axis=-1) + own_weight
    numer = jnp.einsum(
        "skgl,slkd->skgd", weight.astype(jnp.bfloat16), values, preferred_element_type=jnp.float32
    )
    numer = numer + own_weight.astype(jnp.bfloat16).astype(jnp.float32)[..., None] * new_value[
        :, :, None, :
    ].astype(jnp.float32)
    return numer / total[..., None]


def local(
    piece_rows,
    dec_rows,
    norm_gain,
    w_query,
    w_key,
    w_value,
    w_forget,
    forget_bias,
    piece_decay,
    cache_kv,
    cache_gate,
    dec_cache,
    dec_gate,
    dec_lengths,
    w_out,
):
    piece_count = piece_rows.shape[0]
    dec_count = dec_rows.shape[0]
    past_rows = cache_kv.shape[0]
    pairs_here = cache_kv.shape[1]
    head_width = cache_kv.shape[2] // 2
    heads_here = w_forget.shape[1]
    group_size = heads_here // pairs_here
    group_rows = past_rows + piece_count
    normed = norm_rows(jnp.concatenate([piece_rows, dec_rows], axis=0), norm_gain)
    query = jnp.dot(normed, w_query, preferred_element_type=jnp.float32).astype(jnp.bfloat16)
    new_key = jnp.dot(normed, w_key, preferred_element_type=jnp.float32).astype(jnp.bfloat16)
    new_value = jnp.dot(normed, w_value, preferred_element_type=jnp.float32).astype(jnp.bfloat16)
    log_gate = jax.nn.log_sigmoid(
        jnp.dot(normed, w_forget, preferred_element_type=jnp.float32) + forget_bias
    )
    piece_gate = log_gate[:piece_count] + piece_decay.T
    running = jnp.cumsum(piece_gate, axis=0)
    before = carried_in(running[-1], "kv", add_terms, jnp.zeros((heads_here,), jnp.float32))
    new_bias = -(running + before[None, :]).T
    piece_kv = jnp.concatenate(
        [
            new_key[:piece_count].reshape(piece_count, pairs_here, head_width),
            new_value[:piece_count].reshape(piece_count, pairs_here, head_width),
        ],
        axis=-1,
    )
    group_kv = jnp.concatenate([cache_kv, piece_kv], axis=0)
    group_bias = jnp.concatenate([cache_gate, new_bias], axis=1)
    my_group = lax.axis_index("kv")
    every_bias = lax.all_gather(group_bias, "kv", axis=1, tiled=True)
    own_query = query[:piece_count].reshape(piece_count, pairs_here, group_size, head_width)
    own_index = my_group * piece_count + jnp.arange(piece_count, dtype=jnp.int32)
    start_state = (
        jnp.full((piece_count, pairs_here, group_size), -jnp.inf, jnp.float32),
        jnp.zeros((piece_count, pairs_here, group_size), jnp.float32),
        jnp.zeros((piece_count, pairs_here, group_size, head_width), jnp.float32),
    )
    state = start_state
    piece = lax.all_gather(group_kv, "kv", axis=0, tiled=True)
    count = piece.shape[0] // group_rows
    blocks = piece.reshape(count, group_rows, pairs_here, 2 * head_width)

    def visit(carry, item):
        block, offset = item
        bias = lax.dynamic_slice_in_dim(every_bias, offset * group_rows, group_rows, 1)
        part = group_partial(
            own_query,
            own_index,
            block,
            bias.reshape(pairs_here, group_size, group_rows),
            offset,
            past_rows,
            piece_count,
        )
        return (merge_state(carry, part), None)

    state, _ = lax.scan(visit, state, (blocks, jnp.arange(count, dtype=jnp.int32)))
    peak, total, numer = state
    piece_attn = numer / total[..., None]
    dec_attn = decode_attention(
        query[piece_count:].reshape(dec_count, pairs_here, group_size, head_width),
        new_key[piece_count:].reshape(dec_count, pairs_here, head_width),
        new_value[piece_count:].reshape(dec_count, pairs_here, head_width),
        log_gate[piece_count:],
        dec_cache,
        dec_gate,
        dec_lengths,
    )
    attn_rows = jnp.concatenate(
        [
            piece_attn.reshape(piece_count, heads_here * head_width),
            dec_attn.reshape(dec_count, heads_here * head_width),
        ],
        axis=0,
    ).astype(jnp.bfloat16)
    every_head = lax.all_gather(attn_rows, "tp", axis=1, tiled=True)
    mixed = jnp.dot(every_head, w_out, preferred_element_type=jnp.float32).astype(jnp.bfloat16)
    return (mixed[:piece_count], mixed[piece_count:])


def solution(mesh):
    return jax.shard_map(
        local,
        mesh=mesh,
        in_specs=(
            P(("grp", "kv"), None),
            P(("grp", "kv"), None),
            P(),
            P(None, "tp"),
            P(None, "tp"),
            P(None, "tp"),
            P(None, "tp"),
            P("tp"),
            P("tp", ("grp", "kv")),
            P(("grp", "kv"), "tp", None),
            P("tp", ("grp", "kv")),
            P(("grp", "kv"), None, "tp", None),
            P(("grp", "kv"), "tp", None),
            P(("grp", "kv")),
            P(None, "tp"),
        ),
        out_specs=(P(("grp", "kv"), "tp"), P(("grp", "kv"), "tp")),
        check_vma=False,
    )
```

profile of v0, /device:TPU:0, one launch (start us, length us, event | category | flops | bytes accessed | tf_op | source)
XLA Modules:
  0.0 78.9 jit_solution(7893295334877088448)
XLA Ops:
  0.7 0.8 broadcast_add_fusion
  1.5 1.1 %fusion.35 = f32[66]{0:T(128)S(1)} fusion(bf16[2,2048]{1,0:T(2,128)(2,1)} %param.20, bf16[64,2048]{1,0:T(8,128)(2,1)} %param.19), kind=kLoop, calls=%fused_computation.54 | loop fusion | flops 810942 | bytes 270600 | tf_op jit(solution)/shard_map/reduce_sum | solution.py:22
  2.6 1.3 %fusion.42 = f32[66,4]{0,1:T(4,128)S(1)} fusion(bf16[2048,4]{0,1:T(4,128)(2,1)} %param.25, f32[4]{0:T(128)} %param.26, f32[2048]{0:T(1024)} %param.21, f32[66]{0:T(128)S(1)} %add_rsqrt_fusion, bf16[2,2048]{1,0:T(2,128)(2,1)} %param.20, bf16[64,2048]{1,0:T(8,128)(2,1)} %param.19), kind=kOutput, calls=%fused_computation.73 | convolution fusion | flops 2029896 | bytes 296248 | tf_op jit(solution)/shard_map/dot_general | solution.py:125
  3.9 0.7 bitcast_add_fusion
  4.7 1.0 %select_reduce_fusion = f32[2,4]{1,0:T(2,128)S(1)} fusion(f32[2,4,3072]{2,1,0:T(4,128)} %param.31, pred[2,3072]{1,0:T(4,128)(4,1)S(1)} %iota_compare_fusion.1), kind=kLoop, calls=%fused_computation.61 | loop fusion | flops 49144 | bytes 104480 | tf_op jit(solution)/shard_map/reduce_sum | solution.py:68
  5.8 0.7 iota_compare_fusion.2
  6.6 1.4 %convolution_convert_fusion.2 = bf16[66,64]{1,0:T(8,128)(2,1)S(1)} fusion(bf16[2048,64]{0,1:T(8,128)(2,1)} %param.24, f32[2048]{0:T(1024)} %param.21, f32[66]{0:T(128)S(1)} %add_rsqrt_fusion, bf16[2,2048]{1,0:T(2,128)(2,1)} %param.20, bf16[64,2048]{1,0:T(8,128)(2,1)} %param.19), kind=kOutput, calls=%fused_computation.45 | convolution fusion | flops 18251904 | bytes 549384 | tf_op jit(solution)/shard_map/dot_general | solution.py:123
  8.6 12.8 %all-gather = f32[4,1,4]{2,1,0:T(1,128)S(1)} all-gather(f32[1,1,4]{2,1,0:T(1,128)S(1)} %slice_bitcast_fusion.7), channel_id=1, replica_groups=mesh['grp'=2,'kv'=4,'tp'=4] {'kv'}, dimensions={0}, use_global_device_ids=true | all-gather | bytes 80 | tf_op jit(solution)/shard_map/all_gather | solution.py:9
  21.6 1.6 %convolution_convert_fusion.1 = bf16[66,256]{1,0:T(8,128)(2,1)S(1)} fusion(bf16[2048,256]{1,0:T(8,128)(2,1)} %param.22, f32[2048]{0:T(1024)S(1)} %copy-done.8, f32[66]{0:T(128)S(1)} %add_rsqrt_fusion, bf16[2,2048]{1,0:T(2,128)(2,1)S(1)} %copy-done.6, bf16[64,2048]{1,0:T(8,128)(2,1)S(1)} %copy-done.3), kind=kOutput, calls=%fused_computation.44 | convolution fusion | flops 70169088 | bytes 1361160 | tf_op jit(solution)/shard_map/dot_general | solution.py:121
  23.6 13.2 %all-gather.1 = f32[4,832,4]{1,2,0:T(4,128)S(1)} all-gather(f32[1,832,4]{1,2,0:T(4,128)S(1)} %maximum_bitcast_fusion), channel_id=1, replica_groups=mesh['grp'=2,'kv'=4,'tp'=4] {'kv'}, dimensions={0}, use_global_device_ids=true | all-gather | bytes 66560 | tf_op jit(solution)/shard_map/all_gather | solution.py:141
  36.9 0.6 fusion.53
  38.3 0.6 fusion.31
  39.2 17.8 %all_gather.12 = bf16[3328,1,128]{2,0,1:T(8,128)(2,1)S(1)} all-gather(bf16[832,1,128]{2,0,1:T(8,128)(2,1)S(1)} %maximum_maximum_fusion), channel_id=1, replica_groups=mesh['grp'=2,'kv'=4,'tp'=4] {'kv'}, dimensions={0}, use_global_device_ids=true | all-gather | bytes 1064960 | tf_op jit(solution)/shard_map/all_gather | solution.py:150
  57.0 14.4 %while.32 = (s32[]{:T(128)}, f32[64,1,4]{0,2,1:T(4,128)S(1)}, f32[64,1,4]{0,2,1:T(4,128)S(1)}, f32[64,1,4,64]{0,3,2,1:T(8,128)S(1)}, s32[4]{0:T(128)S(1)}, /*ind...) while((s32[]{:T(128)}, f32[64,1,4]{0,2,1:T(4,128)S(1)}, ...), condition=%wide.region_7.8_spmd.clone, body=%wide.region_4.7_spmd.clone.sunk | while | flops 56406536 | bytes 4148079 | solution.py:168
  57.0 0.6 dynamic_slice.41
  59.3 0.4 fusion.69
  59.7 0.3 fusion.71
  60.0 0.5 fusion.73
  60.6 0.6 dynamic_slice.41
  62.9 0.4 fusion.69
  63.3 0.3 fusion.71
  63.6 0.5 fusion.73
  64.2 0.6 dynamic_slice.41
  66.5 0.4 fusion.69
  67.3 0.5 fusion.73
  67.8 0.6 dynamic_slice.41
  70.1 0.4 fusion.69
  70.9 0.5 fusion.73
  71.5 5.8 %all_gather.15 = bf16[66,1024]{0,1:T(8,128)(2,1)S(1)} all-gather(bf16[66,256]{0,1:T(8,128)(2,1)S(1)} %pad_maximum_fusion.1), channel_id=1, replica_groups=mesh['grp'=2,'kv'=4,'tp'=4] {'tp'}, dimensions={1}, use_global_device_ids=true | all-gather | bytes 168960 | tf_op jit(solution)/shard_map/all_gather | solution.py:187
  77.3 0.3 convolution_convert_fusion
  77.7 0.6 slice.76
  78.3 0.6 slice.75
  (104 shorter events, 5.0 us)
Async XLA Ops:
  0.6 76.7 %copy-start = (bf16[1024,512]{1,0:T(8,128)(2,1)S(1)}, bf16[1024,512]{1,0:T(8,128)(2,1)}, u32[]{:S(2)}) copy-start(bf16[1024,512]{1,0:T(8,128)(2,1)} %param.33) | copy-start | bytes 3145732
  0.6 7.3 %copy-start.6 = (bf16[2,2048]{1,0:T(2,128)(2,1)S(1)}, bf16[2,2048]{1,0:T(2,128)(2,1)}, u32[]{:S(2)}) copy-start(bf16[2,2048]{1,0:T(2,128)(2,1)} %param.20) | copy-start | bytes 24580
  0.7 7.3 %copy-start.3 = (bf16[64,2048]{1,0:T(8,128)(2,1)S(1)}, bf16[64,2048]{1,0:T(8,128)(2,1)}, u32[]{:S(2)}) copy-start(bf16[64,2048]{1,0:T(8,128)(2,1)} %param.19) | copy-start | bytes 786436
  0.7 7.3 %copy-start.8 = (f32[2048]{0:T(1024)S(1)}, f32[2048]{0:T(1024)}, u32[]{:S(2)}) copy-start(f32[2048]{0:T(1024)} %param.21) | copy-start | bytes 24580
  0.7 7.3 %copy-start.7 = (bf16[2048,64]{0,1:T(8,128)(2,1)S(1)}, bf16[2048,64]{0,1:T(8,128)(2,1)}, u32[]{:S(2)}) copy-start(bf16[2048,64]{0,1:T(8,128)(2,1)} %param.23) | copy-start | bytes 786436
  2.6 18.9 %copy-start.5 = (f32[4,768]{1,0:T(4,128)S(1)}, f32[4,768]{1,0:T(4,128)}, u32[]{:S(2)}) copy-start(f32[4,768]{1,0:T(4,128)} %param.29) | copy-start | bytes 36868
  8.3 28.6 %copy-start.1 = (bf16[2,3072,1,128]{3,1,2,0:T(8,128)(2,1)S(1)}, bf16[2,3072,1,128]{3,1,2,0:T(8,128)(2,1)}, u32[]{:S(2)}) copy-start(bf16[2,3072,1,128]{3,1,2,0:T(8,128)(2,1)} %param.30) | copy-start | bytes 4718596
  8.3 28.6 %copy-start.2 = (f32[2,4,3072]{2,1,0:T(4,128)S(1)}, f32[2,4,3072]{2,1,0:T(4,128)}, u32[]{:S(2)}) copy-start(f32[2,4,3072]{2,1,0:T(4,128)} %param.31) | copy-start | bytes 294916
  36.9 2.2 %copy-start.4 = (bf16[768,1,128]{2,0,1:T(8,128)(2,1)S(1)}, bf16[768,1,128]{2,0,1:T(8,128)(2,1)}, u32[]{:S(2)}) copy-start(bf16[768,1,128]{2,0,1:T(8,128)(2,1)} %param.28) | copy-start | bytes 589828
where the time goes:
time: 79.3 us; the launch traced here: 78.9 us
  blocking collectives  49.5 us (62%)
  matrix products  9.82 us (12%)
  other arithmetic  6.95 us (9%)
  local copies, waits for them, and re-layouts  6.05 us (8%)
  loops' own time  5.61 us (7%)
  between operations  0.95 us (1%)
    all_gather x1, blocking collectives, local(): piece = lax.all_gather(group_kv, 'kv', axis=0, tiled=True)  17.8 us
    all_gather x1, blocking collectives, local(): every_bias = lax.all_gather(group_bias, 'kv', axis=1, tiled=True)  13.2 us
    all_gather x1, blocking collectives, carried_in(): everything = lax.all_gather(array, axis)  12.8 us
    all_gather x1, blocking collectives, local(): every_head = lax.all_gather(attn_rows, 'tp', axis=1, tiled=True)  5.78 us
    another operation x1, loops' own time, local(): lax.scan(visit, state, (blocks, jnp.arange(count, dtype=jnp.int32)))  5.54 us
    dynamic_slice x12, local copies, waits for them, and re-layouts, local(): lax.scan(visit, state, (blocks, jnp.arange(count, dtype=jnp.int32)))  3.1 us
    dot_general x4, matrix products, group_partial(): jnp.einsum('bkgn,nkd->bkgd', weight.astype(jnp.bfloat16), values, preferr...  2.11 us

commit v1 on v0

v1 whole, which is shorter than its diff:
```python
import functools
import math

import jax
import jax.numpy as jnp
from jax import lax
from jax.experimental import pallas as pl
from jax.experimental.pallas import tpu as pltpu
from jax.sharding import PartitionSpec as P

MESH = pl.DeviceIdType.MESH
LOG2E = math.log2(math.e)
F32 = jnp.float32
BF16 = jnp.bfloat16
HIGH = lax.Precision.HIGHEST


def dot_nt(a, b, precision=None):
    return lax.dot_general(
        a, b, (((1,), (1,)), ((), ())), preferred_element_type=F32, precision=precision
    )


def dot_nn(a, b, precision=None):
    return lax.dot_general(
        a, b, (((1,), (0,)), ((), ())), preferred_element_type=F32, precision=precision
    )


def dot_tn(a, b, precision=None):
    return lax.dot_general(
        a, b, (((0,), (0,)), ((), ())), preferred_element_type=F32, precision=precision
    )


def iota(shape, dim):
    return lax.broadcasted_iota(jnp.int32, shape, dim)


def loop(count, body, carry):
    if count <= 4:
        for k in range(count):
            carry = body(k, carry)
        return carry
    return lax.fori_loop(0, count, body, carry)


def normed_rows(rows, gain):
    wide = rows.astype(F32)
    scale = lax.rsqrt(jnp.mean(wide * wide, axis=-1, keepdims=True) + 1e-06)
    return wide * scale * gain


def kernel(
    n,
    t,
    piece_rows,
    dec_rows,
    gain_in,
    wq_in,
    wk_in,
    wv_in,
    wf_in,
    fb_in,
    decay_in,
    cache_in,
    cgate_in,
    dcache_in,
    dgate_in,
    lens_in,
    wo_in,
    piece_out,
    dec_out,
    rows,
    drows,
    gain,
    wq,
    wkv,
    wf,
    fb,
    decay,
    kv,
    vk,
    cgate,
    dcache,
    dgate,
    lens,
    wo,
    normed,
    qd,
    da,
    qbuf,
    tot,
    part,
    back,
    lse_part,
    lse_back,
    axp,
    axd,
    pbias,
    local_sem,
    q_send,
    q_recv,
    t_send,
    t_recv,
    p_send,
    p_recv,
    l_send,
    l_recv,
    a_send,
    a_recv,
    d_send,
    d_recv,
):
    me = lax.axis_index("kv")
    me_t = lax.axis_index("tp")
    count = piece_rows.shape[0]
    seqs = dec_rows.shape[0]
    past = cache_in.shape[0]
    wide = cache_in.shape[1]
    half = wide // 2
    heads = wf_in.shape[0]
    scale = half ** (-0.5) * LOG2E
    columns = heads * half

    def peer_at(k):
        down = n - 1 - k
        down = jnp.where(down <= me, down - 1, down)
        up = jnp.where(k >= me, k + 1, k)
        return jnp.where(me < n // 2, down, up)

    barrier = pltpu.get_barrier_semaphore()

    def greet(d, _):
        pl.semaphore_signal(
            barrier, inc=1, device_id={"kv": lax.rem(me + d + 1, n)}, device_id_type=MESH
        )
        return 0

    def greet_t(d, _):
        pl.semaphore_signal(
            barrier, inc=1, device_id={"tp": lax.rem(me_t + d + 1, t)}, device_id_type=MESH
        )
        return 0

    loop(n - 1, greet, 0)
    loop(t - 1, greet_t, 0)

    copies = {}
    for k, (name, src, dst) in enumerate(
        (
            ("rows", piece_rows, rows),
            ("drows", dec_rows, drows),
            ("gain", gain_in, gain),
            ("wq", wq_in, wq),
            ("wk", wk_in, wkv.at[pl.ds(0, half)]),
            ("wv", wv_in, wkv.at[pl.ds(half, half)]),
            ("wf", wf_in, wf),
            ("fb", fb_in, fb),
            ("decay", decay_in, decay),
            ("lens", lens_in, lens),
            ("dcache", dcache_in, dcache),
            ("dgate", dgate_in, dgate),
            ("cache", cache_in, kv.at[pl.ds(0, past)]),
            ("cgate", cgate_in, cgate),
            ("wo", wo_in, wo),
        )
    ):
        copy = pltpu.make_async_copy(src, dst, local_sem.at[k])
        copy.start()
        copies[name] = copy

    copies["rows"].wait()
    copies["drows"].wait()
    copies["gain"].wait()
    normed[0:count] = normed_rows(rows[...], gain[...]).astype(BF16)
    dec_normed = normed_rows(drows[...], gain[...])
    spare = normed.shape[0] - count
    normed[count:] = jnp.concatenate(
        [dec_normed, jnp.zeros((spare - seqs, dec_normed.shape[1]), F32)], axis=0
    ).astype(BF16)
    every = normed[...]
    copies["wf"].wait()
    copies["fb"].wait()
    copies["decay"].wait()
    raw = dot_nt(wf[...], every)
    row_of = iota((heads, 1), 0)
    bias = jnp.zeros((heads, 1), F32)
    for h in range(heads):
        bias = jnp.where(row_of == h, fb[h], bias)
    raw = raw + bias
    log_gate = jnp.minimum(raw, 0.0) - jnp.log1p(jnp.exp(-jnp.abs(raw)))
    piece_gate = log_gate[:, 0:count] + decay[...]
    upper = (iota((count, count), 0) <= iota((count, count), 1)).astype(F32)
    running = dot_nn(piece_gate, upper, HIGH)
    tot[0] = jnp.broadcast_to(running[:, count - 1 : count], tot.shape[1:])
    copies["wq"].wait()
    query = dot_nn(every, wq[...]).astype(BF16)
    qbuf[0] = query[0:count]

    pl.semaphore_wait(barrier, n - 1 + t - 1)

    def total_copy(peer):
        slot = lax.rem(peer - me + n, n)
        return pltpu.make_async_remote_copy(
            src_ref=tot.at[0],
            dst_ref=tot.at[slot],
            send_sem=t_send.at[slot],
            recv_sem=t_recv.at[slot],
            device_id={"kv": peer},
            device_id_type=MESH,
        )

    def query_copy(peer):
        slot = lax.rem(peer - me + n, n)
        return pltpu.make_async_remote_copy(
            src_ref=qbuf.at[0],
            dst_ref=qbuf.at[slot],
            send_sem=q_send.at[slot],
            recv_sem=q_recv.at[slot],
            device_id={"kv": peer},
            device_id_type=MESH,
        )

    def send_query(k, _):
        peer = peer_at(k)
        total_copy(peer).start()
        query_copy(peer).start()
        return 0

    loop(n - 1, send_query, 0)

    copies["wk"].wait()
    copies["wv"].wait()
    new_kv = dot_nt(every, wkv[...]).astype(BF16)
    copies["cache"].wait()
    kv[past : past + count] = new_kv[0:count]
    vk[...] = pltpu.roll(kv[...].astype(F32), half, 1).astype(BF16)
    copies["cgate"].wait()
    cgate[...] = cgate[...] * LOG2E

    lanes = seqs * heads
    qd[...] = jnp.zeros(qd.shape, F32)
    dec_query = query[count:].astype(F32)
    for b in range(seqs):
        for h in range(heads):
            qd[b * heads + h : b * heads + h + 1, 0:half] = dec_query[
                b : b + 1, h * half : (h + 1) * half
            ]
    q_dec = qd[...]
    dec_kv = new_kv[count:].astype(F32)
    copies["lens"].wait()
    copies["dgate"].wait()
    copies["dcache"].wait()
    span = dcache.shape[1]
    row = iota((lanes, 1), 0)
    length = jnp.zeros((lanes, 1), jnp.int32)
    own_kv = jnp.zeros((lanes, wide), F32)
    score = jnp.zeros((lanes, span), F32)
    for b in range(seqs):
        mine = (row >= b * heads) & (row < (b + 1) * heads)
        length = jnp.where(mine, lens[b], length)
        own_kv = jnp.where(mine, dec_kv[b : b + 1], own_kv)
        score = jnp.where(mine, dot_nt(q_dec.astype(BF16), dcache[b]), score)
    gate = jnp.concatenate([dgate[b] for b in range(seqs)], axis=0)
    new_gate = jnp.concatenate(
        [log_gate[:, count + b : count + b + 1] for b in range(seqs)], axis=0
    )
    place = iota((lanes, span), 1)
    last = jnp.sum(jnp.where(place == length - 1, gate, 0.0), axis=-1, keepdims=True)
    score = jnp.where(place < length, score * scale - gate * LOG2E, -jnp.inf)
    own = jnp.sum(q_dec * own_kv, axis=-1, keepdims=True) * scale - (last + new_gate) * LOG2E
    peak = jnp.maximum(jnp.max(score, axis=-1, keepdims=True), own)
    weight = jnp.exp2(score - peak)
    own_weight = jnp.exp2(own - peak)
    total = jnp.sum(weight, axis=-1, keepdims=True) + own_weight
    rounded = weight.astype(BF16)
    numer = own_weight.astype(BF16).astype(F32) * own_kv
    for b in range(seqs):
        mine = (row >= b * heads) & (row < (b + 1) * heads)
        numer = numer + jnp.where(mine, dot_nn(rounded, dcache[b]), 0.0)
    numer = numer / total
    da[...] = jnp.zeros(da.shape, F32)
    for b in range(seqs):
        for h in range(heads):
            at = b * heads + h
            da[b : b + 1, h * half : (h + 1) * half] = numer[at : at + 1, half:]
    axd[0] = da[...].astype(BF16)

    def head_copy(d, buf, send, recv):
        return pltpu.make_async_remote_copy(
            src_ref=buf.at[0],
            dst_ref=buf.at[d],
            send_sem=send.at[d],
            recv_sem=recv.at[d],
            device_id={"tp": lax.rem(me_t + d, t)},
            device_id_type=MESH,
        )

    for d in range(1, t):
        head_copy(d, axd, d_send, d_recv).start()

    def add_before(k, before):
        d = k + 1
        total_copy(lax.rem(me + d, n)).wait_recv()
        return before + jnp.where(d <= me, tot[d], 0.0)

    before = loop(n - 1, add_before, jnp.zeros(tot.shape[1:], F32))
    pbias[...] = -(running + before[:, 0:count]) * LOG2E

    low_lane = iota((count, wide), 1) < half
    low = jnp.where(low_lane, 1.0, 0.0).astype(BF16)
    high = jnp.where(low_lane, 0.0, 1.0).astype(BF16)
    lane = iota((count, wide), 1)

    def attend(q, seen):
        pairs = [q[:, p * wide : (p + 1) * wide] for p in range(heads // 2)]
        found = []
        stats = jnp.zeros((count, wide), F32)
        for odd, (mask, keys, values) in enumerate(((low, kv, vk), (high, vk, kv))):
            stacked = jnp.concatenate([p * mask for p in pairs], axis=0)
            old = dot_nt(stacked, keys[0:past])
            new = dot_nt(stacked, keys[past : past + count])
            old_weights, new_weights, sums = [], [], []
            for p in range(heads // 2):
                h = 2 * p + odd
                block = slice(p * count, (p + 1) * count)
                s_old = old[block] * scale + cgate[h : h + 1, :]
                s_new = jnp.where(seen, new[block] * scale + pbias[h : h + 1, :], -jnp.inf)
                top = jnp.maximum(
                    jnp.max(s_old, axis=-1, keepdims=True), jnp.max(s_new, axis=-1, keepdims=True)
                )
                w_old = jnp.exp2(s_old - top)
                w_new = jnp.exp2(s_new - top)
                amount = jnp.sum(w_old, axis=-1, keepdims=True) + jnp.sum(
                    w_new, axis=-1, keepdims=True
                )
                stats = jnp.where(lane == h, top + jnp.log2(amount), stats)
                old_weights.append(w_old.astype(BF16))
                new_weights.append(w_new.astype(BF16))
                sums.append(amount)
            out = dot_nn(jnp.concatenate(old_weights, axis=0), values[0:past])
            out = out + dot_nn(
                jnp.concatenate(new_weights, axis=0), values[past : past + count]
            )
            found.append(
                [out[p * count : (p + 1) * count] / sums[p] for p in range(heads // 2)]
            )
        merged = jnp.concatenate(
            [jnp.where(low_lane, found[0][p], found[1][p]) for p in range(heads // 2)], axis=1
        )
        return merged, jnp.transpose(stats)[0:heads, :]

    def part_copy(peer):
        slot = lax.rem(peer - me + n, n)
        return pltpu.make_async_remote_copy(
            src_ref=part.at[slot],
            dst_ref=back.at[slot],
            send_sem=p_send.at[slot],
            recv_sem=p_recv.at[slot],
            device_id={"kv": peer},
            device_id_type=MESH,
        )

    def lse_copy(peer):
        slot = lax.rem(peer - me + n, n)
        return pltpu.make_async_remote_copy(
            src_ref=lse_part.at[slot],
            dst_ref=lse_back.at[slot],
            send_sem=l_send.at[slot],
            recv_sem=l_recv.at[slot],
            device_id={"kv": peer},
            device_id_type=MESH,
        )

    def serve(k, _):
        peer = peer_at(n - 2 - k)
        came = lax.rem(me - peer + n, n)
        slot = lax.rem(peer - me + n, n)
        query_copy(lax.rem(me + came, n)).wait_recv()
        visible = iota((count, count), 0) * 0 + peer > me
        merged, lse = attend(qbuf[came], visible)
        part[slot] = merged.astype(BF16)
        lse_part[slot] = lse
        part_copy(peer).start()
        lse_copy(peer).start()
        return 0

    loop(n - 1, serve, 0)

    own_part, own_lse = attend(
        qbuf[0], iota((count, count), 1) <= iota((count, count), 0)
    )

    copies["wo"].wait()
    dec_mixed = jnp.zeros((axd.shape[1], wo.shape[1]), F32)
    for d in range(t):
        if d:
            head_copy(d, axd, d_send, d_recv).wait_recv()
        src = lax.rem(me_t - d + t, t)
        depth = pl.ds(pl.multiple_of(src * columns, columns), columns)
        dec_mixed = dec_mixed + dot_nn(axd[d], wo[depth, :])
    dec_out[...] = dec_mixed[0:seqs].astype(BF16)

    def top_of(k, top):
        d = k + 1
        lse_copy(lax.rem(me + d, n)).wait_recv()
        return jnp.maximum(top, lse_back[d])

    top = loop(n - 1, top_of, own_lse)
    own_share = jnp.exp2(own_lse - top)

    def sum_of(k, amount):
        return amount + jnp.exp2(lse_back[k + 1] - top)

    amount = loop(n - 1, sum_of, own_share)
    spread = (
        iota((heads, columns), 1) // half == iota((heads, columns), 0)
    ).astype(F32)

    def add_part(k, acc):
        d = k + 1
        share = dot_tn(jnp.exp2(lse_back[d] - top) / amount, spread, HIGH)
        part_copy(lax.rem(me + d, n)).wait_recv()
        return acc + back[d].astype(F32) * share

    attn = loop(n - 1, add_part, own_part * dot_tn(own_share / amount, spread, HIGH))
    axp[0] = attn.astype(BF16)
    for d in range(1, t):
        head_copy(d, axp, a_send, a_recv).start()
    mixed = jnp.zeros((count, wo.shape[1]), F32)
    for d in range(t):
        if d:
            head_copy(d, axp, a_send, a_recv).wait_recv()
        src = lax.rem(me_t - d + t, t)
        depth = pl.ds(pl.multiple_of(src * columns, columns), columns)
        mixed = mixed + dot_nn(axp[d], wo[depth, :])
    piece_out[...] = mixed.astype(BF16)

    def finish(k, _):
        peer = lax.rem(me + k + 1, n)
        total_copy(peer).wait_send()
        query_copy(peer).wait_send()
        part_copy(peer).wait_send()
        lse_copy(peer).wait_send()
        return 0

    loop(n - 1, finish, 0)
    for d in range(1, t):
        head_copy(d, axd, d_send, d_recv).wait_send()
        head_copy(d, axp, a_send, a_recv).wait_send()


def local(
    n,
    t,
    piece_rows,
    dec_rows,
    norm_gain,
    w_query,
    w_key,
    w_value,
    w_forget,
    forget_bias,
    piece_decay,
    cache_kv,
    cache_gate,
    dec_cache,
    dec_gate,
    dec_lengths,
    w_out,
):
    count, width = piece_rows.shape
    seqs = dec_rows.shape[0]
    past, _, wide = cache_kv.shape
    half = wide // 2
    heads = w_forget.shape[1]
    columns = heads * half
    span = dec_cache.shape[1]
    outs = w_out.shape[1]
    spare = 16
    dma = pltpu.SemaphoreType.DMA
    args = (
        piece_rows,
        dec_rows,
        norm_gain.reshape(1, width),
        w_query,
        w_key.T,
        w_value.T,
        w_forget.T,
        forget_bias,
        piece_decay,
        cache_kv.reshape(past, wide),
        cache_gate,
        dec_cache.reshape(seqs, span, wide),
        dec_gate,
        dec_lengths,
        w_out,
    )
    return pl.pallas_call(
        functools.partial(kernel, n, t),
        out_shape=(
            jax.ShapeDtypeStruct((count, outs), BF16),
            jax.ShapeDtypeStruct((seqs, outs), BF16),
        ),
        in_specs=[pl.BlockSpec(memory_space=pltpu.HBM)] * len(args),
        out_specs=(
            pl.BlockSpec(memory_space=pltpu.VMEM),
            pl.BlockSpec(memory_space=pltpu.VMEM),
        ),
        scratch_shapes=[
            pltpu.VMEM((count, width), BF16),
            pltpu.VMEM((seqs, width), BF16),
            pltpu.VMEM((1, width), F32),
            pltpu.VMEM((width, columns), BF16),
            pltpu.VMEM((wide, width), BF16),
            pltpu.VMEM((heads, width), BF16),
            pltpu.SMEM((heads,), F32),
            pltpu.VMEM((heads, count), F32),
            pltpu.VMEM((past + count, wide), BF16),
            pltpu.VMEM((past + count, wide), BF16),
            pltpu.VMEM((heads, past), F32),
            pltpu.VMEM((seqs, span, wide), BF16),
            pltpu.VMEM((seqs, heads, span), F32),
            pltpu.SMEM((seqs,), jnp.int32),
            pltpu.VMEM(w_out.shape, BF16),
            pltpu.VMEM((count + spare, width), BF16),
            pltpu.VMEM((seqs * heads, wide), F32),
            pltpu.VMEM((spare, columns), F32),
            pltpu.VMEM((n, count, columns), BF16),
            pltpu.VMEM((n, heads, wide), F32),
            pltpu.VMEM((n, count, columns), BF16),
            pltpu.VMEM((n, count, columns), BF16),
            pltpu.VMEM((n, heads, count), F32),
            pltpu.VMEM((n, heads, count), F32),
            pltpu.VMEM((t, count, columns), BF16),
            pltpu.VMEM((t, spare, columns), BF16),
            pltpu.VMEM((heads, count), F32),
            dma((len(args),)),
        ]
        + [dma((n,))] * 8
        + [dma((t,))] * 4,
        compiler_params=pltpu.CompilerParams(collective_id=0, has_side_effects=True),
    )(*args)


def solution(mesh):
    return jax.shard_map(
        functools.partial(local, mesh.shape["kv"], mesh.shape["tp"]),
        mesh=mesh,
        in_specs=(
            P(("grp", "kv"), None),
            P(("grp", "kv"), None),
            P(),
            P(None, "tp"),
            P(None, "tp"),
            P(None, "tp"),
            P(None, "tp"),
            P("tp"),
            P("tp", ("grp", "kv")),
            P(("grp", "kv"), "tp", None),
            P("tp", ("grp", "kv")),
            P(("grp", "kv"), None, "tp", None),
            P(("grp", "kv"), "tp", None),
            P(("grp", "kv")),
            P(None, "tp"),
        ),
        out_specs=(P(("grp", "kv"), "tp"), P(("grp", "kv"), "tp")),
        check_vma=False,
    )
```

time: 79.3 us -> 24.7 us (0.31)
  blocking collectives: 49.5 us -> 0 us
  Pallas kernels: 0 us -> 21.2 us
  matrix products: 9.82 us -> 0 us
  other arithmetic: 6.95 us -> 0 us
  loops' own time: 5.61 us -> 0 us
  local copies, waits for them, and re-layouts: 6.05 us -> 2.72 us
    all_gather x4 -> x0, blocking collectives: 49.5 us -> none  [the longest x1 17.8 us: local(): piece = lax.all_gather(group_kv, 'kv', axis=0, tiled=True)]
    pallas_call x0 -> x1, Pallas kernels: none -> 21.2 us  [local(): pl.pallas_call(functools.partial(kernel, n, t), out_shape=(jax.ShapeDtype...]
    dot_general x16 -> x0, matrix products: 9.82 us -> none  [the longest x4 2.11 us: group_partial(): jnp.einsum('bkgn,nkd->bkgd', weight.astype(jnp.bfloat16), values, preferr...]
    another operation x2 -> x0, loops' own time: 5.61 us -> none  [the longest x1 5.54 us: local(): lax.scan(visit, state, (blocks, jnp.arange(count, dtype=jnp.int32)))]
    reduce_sum x7 -> x0, other arithmetic: 3.58 us -> none  [the longest x4 1.21 us: group_partial(): total = jnp.sum(weight, axis=-1)]
    dynamic_slice x16 -> x0, local copies, waits for them, and re-layouts: 3.43 us -> none  [the longest x12 3.1 us: local(): lax.scan(visit, state, (blocks, jnp.arange(count, dtype=jnp.int32)))]
    unnamed x21 -> x2, local copies, waits for them, and re-layouts: 0.19 us -> 2.72 us
    slice x5 -> x0, local copies, waits for them, and re-layouts: 1.24 us -> none  [the longest x2 1.22 us: local(): return (mixed[:piece_count], mixed[piece_count:])]
where the time goes in v1:
time: 24.7 us; the launch traced here: 24.5 us
  Pallas kernels  21.2 us (86%)
  local copies, waits for them, and re-layouts  2.72 us (11%)
  between operations  0.64 us (3%)
    pallas_call x1, Pallas kernels, local(): pl.pallas_call(functools.partial(kernel, n, t), out_shape=(jax.ShapeDtype...  21.2 us
    unnamed x2, local copies, waits for them, and re-layouts  2.72 us

profile of v1, /device:TPU:0, one launch (start us, length us, event | category | flops | bytes accessed | tf_op | source)
XLA Modules:
  0.0 24.5 jit_solution(13460555193428500021)
XLA Ops:
  0.6 21.2 %shard_map.158 = (bf16[64,512]{1,0:T(8,128)(2,1)}, bf16[2,512]{1,0:T(2,128)(2,1)}) custom-call(bf16[64,2048]{1,0:T(8,128)(2,1)} %piece_rows.1, bf16[2,2048]{1,0:T(2,128)(2,1)} %dec_rows.1, f32[1,2048]{1,0:T(1,128)} %bitcast.11, bf16[2048,256]{1,0:T(8,128)(2,1)} %wq_in.1, bf16[64,2048]{1,0:T(8,128)(2,1)} %bitcast.7, bf16[64,2048]{1,0:T(8,128)(2,1)} %bitcast.8, ...), custom_call_target="tpu_custom_call" | custom-call | tf_op jit(solution)/shard_map/pallas_call | solution.py:500
  21.8 1.5 %copy.19 = bf16[64,512]{1,0:T(8,128)(2,1)} copy(bf16[64,512]{1,0:T(8,128)(2,1)} %get-tuple-element.4) | data formatting | bytes 131072
  23.3 1.2 %copy.20 = bf16[2,512]{1,0:T(2,128)(2,1)} copy(bf16[2,512]{1,0:T(2,128)(2,1)} %get-tuple-element.5) | data formatting | bytes 4096

commit v2 on v1

--- a/solution.py
+++ b/solution.py
@@ -451,6 +451,15 @@
         head_copy(d, axp, a_send, a_recv).wait_send()
 
 
+def write_out(piece_in, dec_in, piece_out, dec_out, sem):
+    first = pltpu.make_async_copy(piece_in, piece_out, sem.at[0])
+    second = pltpu.make_async_copy(dec_in, dec_out, sem.at[1])
+    first.start()
+    second.start()
+    first.wait()
+    second.wait()
+
+
 def local(
     n,
     t,
@@ -497,7 +506,8 @@
         dec_lengths,
         w_out,
     )
-    return pl.pallas_call(
+    args = tuple(pltpu.with_memory_space_constraint(a, pltpu.HBM) for a in args)
+    mixed = pl.pallas_call(
         functools.partial(kernel, n, t),
         out_shape=(
             jax.ShapeDtypeStruct((count, outs), BF16),
@@ -540,8 +550,18 @@
         ]
         + [dma((n,))] * 8
         + [dma((t,))] * 4,
-        compiler_params=pltpu.CompilerParams(collective_id=0, has_side_effects=True),
+        compiler_params=pltpu.CompilerParams(
+            collective_id=0, has_side_effects=True, vmem_limit_bytes=24 * 1024 * 1024
+        ),
     )(*args)
+    return pl.pallas_call(
+        write_out,
+        out_shape=tuple(jax.ShapeDtypeStruct(m.shape, m.dtype) for m in mixed),
+        in_specs=[pl.BlockSpec(memory_space=pltpu.VMEM)] * 2,
+        out_specs=(pl.BlockSpec(memory_space=pltpu.HBM),) * 2,
+        scratch_shapes=[dma((2,))],
+        compiler_params=pltpu.CompilerParams(vmem_limit_bytes=4 * 1024 * 1024),
+    )(*mixed)
 
 
 def solution(mesh):

time: 24.7 us -> 22 us (0.89)
  local copies, waits for them, and re-layouts: 2.72 us -> 0 us
    unnamed x2 -> x0, local copies, waits for them, and re-layouts: 2.72 us -> none
    pallas_call x0 -> x1, Pallas kernels: none -> 0.65 us  [local(): pl.pallas_call(write_out, out_shape=tuple((jax.ShapeDtypeStruct(m.shape,...]
    pallas_call x1, Pallas kernels: 21.2 us -> 20.6 us  [local(): pl.pallas_call(functools.partial(kernel, n, t), out_shape=(jax.ShapeDtype...]
where the time goes in v2:
time: 22 us; the launch traced here: 21.9 us
  Pallas kernels  21.2 us (96%)
  between operations  0.64 us (3%)
    pallas_call x1, Pallas kernels, local(): pl.pallas_call(functools.partial(kernel, n, t), out_shape=(jax.ShapeDtype...  20.6 us
    pallas_call x1, Pallas kernels, local(): pl.pallas_call(write_out, out_shape=tuple((jax.ShapeDtypeStruct(m.shape,...  0.65 us

profile of v2, /device:TPU:0, one launch (start us, length us, event | category | flops | bytes accessed | tf_op | source)
XLA Modules:
  0.0 21.9 jit_solution(11103372153320141060)
XLA Ops:
  0.6 20.6 %shard_map.158 = (bf16[64,512]{1,0:T(8,128)(2,1)S(1)}, bf16[2,512]{1,0:T(2,128)(2,1)S(1)}) custom-call(bf16[64,2048]{1,0:T(8,128)(2,1)} %piece_rows.1, bf16[2,2048]{1,0:T(2,128)(2,1)} %dec_rows.1, f32[1,2048]{1,0:T(1,128)} %bitcast.11, bf16[2048,256]{1,0:T(8,128)(2,1)} %wq_in.1, bf16[64,2048]{1,0:T(8,128)(2,1)} %bitcast.7, bf16[64,2048]{1,0:T(8,128)(2,1)} %bitcast.8, ...), custom_call_target="tpu_custom_call" | custom-call | tf_op jit(solution)/shard_map/pallas_call | solution.py:510
  21.2 0.7 %shard_map.159 = (bf16[64,512]{1,0:T(8,128)(2,1)}, bf16[2,512]{1,0:T(2,128)(2,1)}) custom-call(bf16[64,512]{1,0:T(8,128)(2,1)S(1)} %get-tuple-element.4.piece_in, bf16[2,512]{1,0:T(2,128)(2,1)S(1)} %get-tuple-element.5.dec_in), custom_call_target="tpu_custom_call" | custom-call | tf_op jit(solution)/shard_map/pallas_call | solution.py:557

commit v3 on v2

--- a/solution.py
+++ b/solution.py
@@ -167,12 +167,17 @@
         )
     ):
         copy = pltpu.make_async_copy(src, dst, local_sem.at[k])
-        copy.start()
         copies[name] = copy
+    late = ("dcache", "dgate", "cache", "cgate", "wo")
+    for name, copy in copies.items():
+        if name not in late:
+            copy.start()
 
     copies["rows"].wait()
     copies["drows"].wait()
     copies["gain"].wait()
+    for name in late:
+        copies[name].start()
     normed[0:count] = normed_rows(rows[...], gain[...]).astype(BF16)
     dec_normed = normed_rows(drows[...], gain[...])
     spare = normed.shape[0] - count
@@ -182,7 +187,10 @@
     every = normed[...]
     copies["wf"].wait()
     copies["fb"].wait()
+    copies["wq"].wait()
     copies["decay"].wait()
+    query = dot_nn(every, wq[...]).astype(BF16)
+    qbuf[0] = query[0:count]
     raw = dot_nt(wf[...], every)
     row_of = iota((heads, 1), 0)
     bias = jnp.zeros((heads, 1), F32)
@@ -194,9 +202,6 @@
     upper = (iota((count, count), 0) <= iota((count, count), 1)).astype(F32)
     running = dot_nn(piece_gate, upper, HIGH)
     tot[0] = jnp.broadcast_to(running[:, count - 1 : count], tot.shape[1:])
-    copies["wq"].wait()
-    query = dot_nn(every, wq[...]).astype(BF16)
-    qbuf[0] = query[0:count]
 
     pl.semaphore_wait(barrier, n - 1 + t - 1)
 
@@ -380,10 +385,10 @@
         query_copy(lax.rem(me + came, n)).wait_recv()
         visible = iota((count, count), 0) * 0 + peer > me
         merged, lse = attend(qbuf[came], visible)
+        lse_part[slot] = lse
+        lse_copy(peer).start()
         part[slot] = merged.astype(BF16)
-        lse_part[slot] = lse
         part_copy(peer).start()
-        lse_copy(peer).start()
         return 0
 
     loop(n - 1, serve, 0)

time: 22 us -> 21.6 us (0.982)
  Pallas kernels: 21.2 us -> 20.8 us
    pallas_call x1, Pallas kernels: 20.6 us -> 20.1 us  [local(): pl.pallas_call(functools.partial(kernel, n, t), out_shape=(jax.ShapeDtype...]
where the time goes in v3:
time: 21.6 us; the launch traced here: 21.4 us
  Pallas kernels  20.8 us (96%)
  between operations  0.64 us (3%)
    pallas_call x1, Pallas kernels, local(): pl.pallas_call(functools.partial(kernel, n, t), out_shape=(jax.ShapeDtype...  20.1 us
    pallas_call x1, Pallas kernels, local(): pl.pallas_call(write_out, out_shape=tuple((jax.ShapeDtypeStruct(m.shape,...  0.65 us

profile of v3, /device:TPU:0, one launch (start us, length us, event | category | flops | bytes accessed | tf_op | source)
XLA Modules:
  0.0 21.4 jit_solution(6496595939369406220)
XLA Ops:
  0.6 20.1 %shard_map.158 = (bf16[64,512]{1,0:T(8,128)(2,1)S(1)}, bf16[2,512]{1,0:T(2,128)(2,1)S(1)}) custom-call(bf16[64,2048]{1,0:T(8,128)(2,1)} %piece_rows.1, bf16[2,2048]{1,0:T(2,128)(2,1)} %dec_rows.1, f32[1,2048]{1,0:T(1,128)} %bitcast.11, bf16[2048,256]{1,0:T(8,128)(2,1)} %wq_in.1, bf16[64,2048]{1,0:T(8,128)(2,1)} %bitcast.7, bf16[64,2048]{1,0:T(8,128)(2,1)} %bitcast.8, ...), custom_call_target="tpu_custom_call" | custom-call | tf_op jit(solution)/shard_map/pallas_call | solution.py:515
  20.8 0.7 %shard_map.159 = (bf16[64,512]{1,0:T(8,128)(2,1)}, bf16[2,512]{1,0:T(2,128)(2,1)}) custom-call(bf16[64,512]{1,0:T(8,128)(2,1)S(1)} %get-tuple-element.4.piece_in, bf16[2,512]{1,0:T(2,128)(2,1)S(1)} %get-tuple-element.5.dec_in), custom_call_target="tpu_custom_call" | custom-call | tf_op jit(solution)/shard_map/pallas_call | solution.py:562
